TPU v7x, 32 devices: a whole 2x2x4 slice. The times are simulated.
32 devices in a mesh: kv: 8 (over z, y), tp: 4 (over x, core).
Axes of the slice: x: 2, y: 2, z: 4, core: 2. Of those that a mesh axis runs over, the one named last changes fastest.
Arguments:
- tokens: bfloat16 [128, 4096], P('tp', 'kv')
- seq_pos: int32 [128], P('kv'), may hold values from 0 to 4095
- state: float32 [128, 16, 128, 256], P('kv', 'tp'), may hold values from -0.6 to 0.6
- norm_in_gain: float32 [4096], P('kv'), may hold values from 0.1 to 1.9
- query_weight: bfloat16 [4096, 2048], P('kv', 'tp'), may hold values from -0.09375 to 0.09375
- key_weight: bfloat16 [4096, 2048], P('kv', 'tp'), may hold values from -0.09375 to 0.09375
- value_weight: bfloat16 [4096, 4096], P('kv', 'tp'), may hold values from -0.09375 to 0.09375
- gate_weight: bfloat16 [4096, 4096], P('kv', 'tp'), may hold values from -0.09375 to 0.09375
- head_gain: float32 [4096], P('tp'), may hold values from 0.1 to 1.9
- out_weight: bfloat16 [4096, 4096], P('tp', 'kv'), may hold values from -0.09375 to 0.09375
- norm_mlp_gain: float32 [4096], P('kv'), may hold values from 0.1 to 1.9
- hidden_weight: bfloat16 [4096, 16384], P('kv', 'tp'), may hold values from -0.09375 to 0.09375
- down_weight: bfloat16 [16384, 4096], P('tp', 'kv'), may hold values from -0.046875 to 0.046875
Outputs:
- output: bfloat16 [128, 4096], P('tp', 'kv')
- new_state: float32 [128, 16, 128, 256], P('kv', 'tp')
All inputs are finite; a program needn't handle non-finite values.
Results may differ from a plain program's by a relative error of at most 0.03.
Values may be sent and summed in bfloat16 or wider, within the bound.
A program may use at most 64 MiB of HBM per device.

v0:
```python
import jax
import jax.numpy as jnp
from jax import lax
from jax.sharding import PartitionSpec as P

D = 4096
H = 16
DK = 128
DV = 256
EPS = 1e-06


def rotate(vectors, positions):
    half = vectors.shape[-1] // 2
    inverse = jnp.power(10000.0, -jnp.arange(half, dtype=jnp.float32) / half)
    angles = positions.astype(jnp.float32)[:, None] * inverse[None, :]
    cosine = jnp.cos(angles)[:, None, :]
    sine = jnp.sin(angles)[:, None, :]
    first, second = (vectors[..., :half], vectors[..., half:])
    return jnp.concatenate(
        [first * cosine - second * sine, first * sine + second * cosine], axis=-1
    )


def head_decay(head_ids):
    return 1.0 - jnp.exp2(-2.0 - 6.0 * head_ids / (H - 1))


def local(
    tokens,
    seq_pos,
    state,
    norm_in_gain,
    query_weight,
    key_weight,
    value_weight,
    gate_weight,
    head_gain,
    out_weight,
    norm_mlp_gain,
    hidden_weight,
    down_weight,
):
    rows_all = lax.all_gather(tokens, "tp", axis=0, tiled=True)
    rows_f = rows_all.astype(jnp.float32)
    squares_in = jnp.sum(rows_f * rows_f, axis=1)
    normed_in = (rows_f * norm_in_gain[None, :]).astype(jnp.bfloat16)
    term_query = jnp.dot(normed_in, query_weight, preferred_element_type=jnp.float32).astype(
        jnp.bfloat16
    )
    term_keys = jnp.dot(normed_in, key_weight, preferred_element_type=jnp.float32).astype(
        jnp.bfloat16
    )
    term_values = jnp.dot(normed_in, value_weight, preferred_element_type=jnp.float32).astype(
        jnp.bfloat16
    )
    term_gates = jnp.dot(normed_in, gate_weight, preferred_element_type=jnp.float32).astype(
        jnp.bfloat16
    )
    total_all = lax.psum(squares_in, "kv")
    query, keys, values, gates = (
        lax.psum_scatter(term_query, "kv", scatter_dimension=0, tiled=True).astype(jnp.float32),
        lax.psum_scatter(term_keys, "kv", scatter_dimension=0, tiled=True).astype(jnp.float32),
        lax.psum_scatter(term_values, "kv", scatter_dimension=0, tiled=True).astype(jnp.float32),
        lax.psum_scatter(term_gates, "kv", scatter_dimension=0, tiled=True).astype(jnp.float32),
    )
    own_rows = query.shape[0]
    total_in = lax.dynamic_slice_in_dim(total_all, lax.axis_index("kv") * own_rows, own_rows, 0)
    factor = lax.rsqrt(total_in / D + EPS)[:, None]
    query, keys, values, gates = (query * factor, keys * factor, values * factor, gates * factor)
    local_rows = query.shape[0]
    heads_dev = H // lax.axis_size("tp")
    turned_query = rotate(query.reshape(local_rows, heads_dev, DK), seq_pos)
    turned_keys = rotate(keys.reshape(local_rows, heads_dev, DK), seq_pos) * DK ** (-0.5)
    head_ids = (lax.axis_index("tp") * heads_dev + jnp.arange(heads_dev, dtype=jnp.int32)).astype(
        jnp.float32
    )
    decay = head_decay(head_ids)
    new_state = decay[None, :, None, None] * state + jnp.einsum(
        "bhk,bhv->bhkv",
        turned_keys,
        values.reshape(local_rows, heads_dev, DV),
        precision=lax.Precision.HIGHEST,
    )
    read = jnp.einsum("bhk,bhkv->bhv", turned_query, new_state, precision=lax.Precision.HIGHEST)
    read = read * lax.rsqrt(jnp.mean(read * read, axis=-1, keepdims=True) + EPS)
    mixed = (
        read.reshape(local_rows, heads_dev * DV) * head_gain[None, :] * jax.nn.silu(gates)
    ).astype(jnp.bfloat16)
    attn_terms = jnp.dot(
        lax.all_gather(mixed, "kv", axis=0, tiled=True),
        out_weight,
        preferred_element_type=jnp.float32,
    )
    attn = lax.psum_scatter(
        attn_terms.astype(jnp.bfloat16), "tp", scatter_dimension=0, tiled=True
    ).astype(jnp.float32)
    resid = (tokens.astype(jnp.float32) + attn).astype(jnp.bfloat16)
    resid_all = lax.all_gather(resid, "tp", axis=0, tiled=True)
    resid_f = resid_all.astype(jnp.float32)
    squares_mid = jnp.sum(resid_f * resid_f, axis=1)
    normed_mid = (resid_f * norm_mlp_gain[None, :]).astype(jnp.bfloat16)
    term_hidden = jnp.dot(normed_mid, hidden_weight, preferred_element_type=jnp.float32).astype(
        jnp.bfloat16
    )
    total_mid = lax.psum(squares_mid, "kv")
    scale_mid = lax.rsqrt(total_mid / D + EPS)[:, None]
    hidden = lax.psum(term_hidden, "kv").astype(jnp.float32)
    active = jnp.square(jax.nn.relu(hidden * scale_mid)).astype(jnp.bfloat16)
    down_terms = jnp.dot(active, down_weight, preferred_element_type=jnp.float32)
    down = lax.psum_scatter(
        down_terms.astype(jnp.bfloat16), "tp", scatter_dimension=0, tiled=True
    ).astype(jnp.float32)
    output = (resid.astype(jnp.float32) + down).astype(jnp.bfloat16)
    return (output, new_state)


def solution(mesh):
    placed = (
        P("tp", "kv"),
        P("kv"),
        P("kv", "tp", None, None),
        P("kv"),
        P("kv", "tp"),
        P("kv", "tp"),
        P("kv", "tp"),
        P("kv", "tp"),
        P("tp"),
        P("tp", "kv"),
        P("kv"),
        P("kv", "tp"),
        P("tp", "kv"),
    )
    return jax.shard_map(
        local,
        mesh=mesh,
        in_specs=placed,
        out_specs=(P("tp", "kv"), P("kv", "tp", None, None)),
        check_vma=False,
    )
```

profile of v0, /device:TPU:0, one launch (start us, length us, event | category | flops | bytes accessed | tf_op | source)
XLA Modules:
  0.0 445.5 jit_solution(3664040884219889815)
XLA Ops:
  7.2 6.9 %all_gather.9 = bf16[128,512]{1,0:T(8,128)(2,1)S(1)} all-gather(bf16[32,512]{1,0:T(8,128)(2,1)} %param.13), channel_id=1, replica_groups=mesh['kv'=8,'tp'=4] {'tp'}, dimensions={0}, use_global_device_ids=true | all-gather | bytes 163840 | tf_op jit(solution)/shard_map/all_gather | solution.py:44
  14.1 2.0 convolution_convert_fusion.4
  16.1 1.9 convolution_convert_fusion.5
  18.1 1.7 convolution_convert_fusion.2
  19.9 2.2 convolution_convert_fusion.1
  22.3 0.1 fusion.3
  22.4 22.1 %psum.21 = f32[128]{0:T(128)S(1)} all-reduce(f32[128]{0:T(128)S(1)} %fusion.3), channel_id=1, replica_groups=mesh['kv'=8,'tp'=4] {'kv'}, use_global_device_ids=true, to_apply=%region_2.0 | all-reduce | flops 128 | bytes 1024 | tf_op jit(solution)/shard_map/psum | solution.py:60
  44.5 0.1 multiply_cosine_fusion
  44.7 35.0 %reduce-scatter.9.cloned.1.call-done = bf16[16,512]{1,0:T(8,128)(2,1)} async-done(((bf16[128,512]{1,0:T(8,128)(2,1)}), bf16[16,512]{1,0:T(8,128)(2,1)}) %reduce-scatter.9.cloned.1.call-update) | async-done | bytes 16400 | tf_op jit(solution)/shard_map/reduce_scatter | solution.py:63
  79.7 64.2 %reduce-scatter.7.cloned.1.call-done = bf16[16,512]{1,0:T(8,128)(2,1)} async-done(((bf16[128,512]{1,0:T(8,128)(2,1)}), bf16[16,512]{1,0:T(8,128)(2,1)}) %reduce-scatter.7.cloned.1.call-update) | async-done | bytes 16400 | tf_op jit(solution)/shard_map/reduce_scatter | solution.py:62
  143.9 0.8 convert_multiply_fusion.5
  144.7 0.1 multiply_subtract_fusion
  144.8 0.1 pad_maximum_fusion
  144.9 64.0 %reduce-scatter.11.cloned.1.call-done = bf16[16,1024]{1,0:T(8,128)(2,1)} async-done(((bf16[128,1024]{1,0:T(8,128)(2,1)}), bf16[16,1024]{1,0:T(8,128)(2,1)}) %reduce-scatter.11.cloned.1.call-update) | async-done | bytes 32784 | tf_op jit(solution)/shard_map/reduce_scatter | solution.py:64
  208.9 0.8 convert_multiply_fusion.4
  209.7 4.1 multiply_add_fusion
  213.9 4.1 fusion.14
  218.0 0.1 fusion.12
  218.3 55.3 %reduce-scatter.13.cloned.1.call-done = bf16[16,1024]{1,0:T(8,128)(2,1)} async-done(((bf16[128,1024]{1,0:T(8,128)(2,1)}), bf16[16,1024]{1,0:T(8,128)(2,1)}) %reduce-scatter.13.cloned.1.call-update) | async-done | bytes 32784 | tf_op jit(solution)/shard_map/reduce_scatter | solution.py:65
  273.6 0.9 multiply_convert_fusion.2
  274.4 30.9 %all_gather.10 = bf16[128,1024]{1,0:T(8,128)(2,1)S(1)} all-gather(bf16[16,1024]{1,0:T(8,128)(2,1)S(1)} %multiply_convert_fusion.2), channel_id=1, replica_groups=mesh['kv'=8,'tp'=4] {'kv'}, dimensions={0}, use_global_device_ids=true | all-gather | bytes 294912 | tf_op jit(solution)/shard_map/all_gather | solution.py:91
  305.3 1.0 convolution_convert_fusion.6
  306.4 18.8 %reduce-scatter.15.cloned.1.call-done = bf16[32,512]{1,0:T(8,128)(2,1)} async-done(((bf16[128,512]{1,0:T(8,128)(2,1)}), bf16[32,512]{1,0:T(8,128)(2,1)}) %reduce-scatter.15.cloned.1.call-update) | async-done | bytes 32784 | tf_op jit(solution)/shard_map/reduce_scatter | solution.py:95
  325.2 0.8 add_convert_fusion.1
  325.9 5.4 %all_gather.11 = bf16[128,512]{1,0:T(8,128)(2,1)S(1)} all-gather(bf16[32,512]{1,0:T(8,128)(2,1)S(1)} %add_convert_fusion.1), channel_id=1, replica_groups=mesh['kv'=8,'tp'=4] {'tp'}, dimensions={0}, use_global_device_ids=true | all-gather | bytes 163840 | tf_op jit(solution)/shard_map/all_gather | solution.py:99
  331.3 3.9 convolution_convert_fusion
  335.4 0.1 fusion.5
  335.5 21.6 %psum.23 = f32[128]{0:T(128)S(1)} all-reduce(f32[128]{0:T(128)S(1)} %fusion.5), channel_id=1, replica_groups=mesh['kv'=8,'tp'=4] {'kv'}, use_global_device_ids=true, to_apply=%region_10.11 | all-reduce | flops 128 | bytes 1024 | tf_op jit(solution)/shard_map/psum | solution.py:106
  357.1 56.9 %all-reduce.2.cloned.1.call-done = bf16[128,4096]{1,0:T(8,128)(2,1)} async-done(((bf16[128,4096]{1,0:T(8,128)(2,1)}), bf16[128,4096]{1,0:T(8,128)(2,1)}) %all-reduce.2.cloned.1.call-update) | async-done | bytes 1048592 | tf_op jit(solution)/shard_map/psum | solution.py:108
  414.0 3.9 convolution_convert_fusion.3
  417.9 19.4 %reduce-scatter.17.cloned.1.call-done = bf16[32,512]{1,0:T(8,128)(2,1)} async-done(((bf16[128,512]{1,0:T(8,128)(2,1)}), bf16[32,512]{1,0:T(8,128)(2,1)}) %reduce-scatter.17.cloned.1.call-update) | async-done | bytes 32784 | tf_op jit(solution)/shard_map/reduce_scatter | solution.py:111
  437.3 1.4 add_convert_fusion
  (39 shorter events, 0.7 us)
Async XLA Ops:
  7.2 11.0 %copy-start = (bf16[512,1024]{1,0:T(8,128)(2,1)S(1)}, bf16[512,1024]{1,0:T(8,128)(2,1)}, u32[]{:S(2)}) copy-start(bf16[512,1024]{1,0:T(8,128)(2,1)} %param.19) | copy-start | bytes 3145732
  7.2 15.2 %copy-start.6 = (s32[16]{0:T(128)S(1)}, s32[16]{0:T(128)}, u32[]{:S(2)}) copy-start(s32[16]{0:T(128)} %param.14) | copy-start | bytes 196
  7.2 72.5 %reduce-scatter.9.cloned.1.call-start = ((), (), s32[]{:S(2)}) async-start(), calls=%async_computation.7 | async-start | bytes 147456 | tf_op jit(solution)/shard_map/reduce_scatter | solution.py:63
  16.1 127.8 %reduce-scatter.7.cloned.1.call-start = ((), (), s32[]{:S(2)}) async-start(), calls=%async_computation.6 | async-start | bytes 147456 | tf_op jit(solution)/shard_map/reduce_scatter | solution.py:62
  18.1 190.8 %reduce-scatter.11.cloned.1.call-start = ((), (), s32[]{:S(2)}) async-start(), calls=%async_computation.8 | async-start | bytes 294912 | tf_op jit(solution)/shard_map/reduce_scatter | solution.py:64
  19.9 253.7 %reduce-scatter.13.cloned.1.call-start = ((), (), s32[]{:S(2)}) async-start(), calls=%async_computation.9 | async-start | bytes 294912 | tf_op jit(solution)/shard_map/reduce_scatter | solution.py:65
  22.2 303.0 %reduce-scatter.15.cloned.1.call-start = ((), (), s32[]{:S(2)}) async-start(), calls=%async_computation.10 | async-start | bytes 163840 | tf_op jit(solution)/shard_map/reduce_scatter | solution.py:95
  213.9 4.1 copy-start.1
  213.9 59.7 %copy-start.4 = (f32[1024]{0:T(1024)S(1)}, f32[1024]{0:T(1024)}, u32[]{:S(2)}) copy-start(f32[1024]{0:T(1024)} %param.21) | copy-start | bytes 12292
  213.9 91.4 %copy-start.2 = (bf16[1024,512]{1,0:T(8,128)(2,1)S(1)}, bf16[1024,512]{1,0:T(8,128)(2,1)}, u32[]{:S(2)}) copy-start(bf16[1024,512]{1,0:T(8,128)(2,1)} %param.22) | copy-start | bytes 3145732
  213.9 111.2 %copy-start.3 = (bf16[32,512]{1,0:T(8,128)(2,1)S(1)}, bf16[32,512]{1,0:T(8,128)(2,1)}, u32[]{:S(2)}) copy-start(bf16[32,512]{1,0:T(8,128)(2,1)} %param.13) | copy-start | bytes 98308
  213.9 117.4 %copy-start.5 = (f32[512]{0:T(512)S(1)}, f32[512]{0:T(512)}, u32[]{:S(2)}) copy-start(f32[512]{0:T(512)} %param.23) | copy-start | bytes 6148
  306.3 107.6 %all-reduce.2.cloned.1.call-start = ((), (), s32[]{:S(2)}) async-start(), calls=%async_computation.11 | async-start | bytes 2097152 | tf_op jit(solution)/shard_map/psum | solution.py:108
  335.3 102.0 %reduce-scatter.17.cloned.1.call-start = ((), (), s32[]{:S(2)}) async-start(), calls=%async_computation.12 | async-start | bytes 163840 | tf_op jit(solution)/shard_map/reduce_scatter | solution.py:111
Sparse Core Ops, SparseCore 0:
  16.2 63.4 reduce-scatter.8
  83.0 60.8 reduce-scatter.6
  147.8 61.0 reduce-scatter.10
  212.1 61.4 reduce-scatter.12
  306.5 18.6 reduce-scatter.14
  335.4 78.4 all-reduce.1
  418.0 19.2 reduce-scatter.16
where the time goes:
time: 446 us
  waiting for transfers between devices  314 us (70%)
  blocking collectives  86.9 us (19%)
  matrix products  20.8 us (5%)
  between operations  14.3 us (3%)
  other arithmetic  9.62 us (2%)
    reduce_scatter x1, waiting for transfers between devices, local(): lax.psum_scatter(term_query, 'kv', scatter_dimension=0, tiled=True)  64.2 us
    reduce_scatter x1, waiting for transfers between devices, local(): lax.psum_scatter(term_values, 'kv', scatter_dimension=0, tiled=True)  64 us
    psum x1, waiting for transfers between devices, local(): hidden = lax.psum(term_hidden, 'kv').astype(jnp.float32)  56.9 us
    reduce_scatter x1, waiting for transfers between devices, local(): lax.psum_scatter(term_gates, 'kv', scatter_dimension=0, tiled=True)  55.3 us
    reduce_scatter x1, waiting for transfers between devices, local(): lax.psum_scatter(term_keys, 'kv', scatter_dimension=0, tiled=True)  35 us
    all_gather x1, blocking collectives, local(): lax.all_gather(mixed, 'kv', axis=0, tiled=True)  30.9 us
    psum x1, blocking collectives, local(): total_all = lax.psum(squares_in, 'kv')  22.1 us
    psum x1, blocking collectives, local(): total_mid = lax.psum(squares_mid, 'kv')  21.6 us
  transfers between devices with their start and end apart: 7, of which 7 were waited for; matrix products, arithmetic and copies ran while one was open for 4% of the time, Pallas kernels for 0%

commit v1 on v0

--- a/solution.py
+++ b/solution.py
@@ -88,7 +88,15 @@
         read.reshape(local_rows, heads_dev * DV) * head_gain[None, :] * jax.nn.silu(gates)
     ).astype(jnp.bfloat16)
     attn_terms = jnp.dot(
-        lax.all_gather(mixed, "kv", axis=0, tiled=True),
+        jnp.concatenate(
+            lax.all_to_all(
+                jnp.stack([mixed for _ in range(lax.axis_size("kv"))], axis=0),
+                axis_name="kv",
+                split_axis=0,
+                concat_axis=0,
+            ),
+            axis=0,
+        ),
         out_weight,
         preferred_element_type=jnp.float32,
     )

time: 446 us -> 426 us (0.955)
  blocking collectives: 86.9 us -> 67.6 us
    all_gather x1 -> x0, blocking collectives: 30.9 us -> none  [local(): lax.all_gather(mixed, 'kv', axis=0, tiled=True)]
    all_to_all x0 -> x1, blocking collectives: none -> 11.7 us  [local(): lax.all_to_all(jnp.stack([mixed for _ in range(lax.axis_size('kv'))], axi...]
where the time goes in v1:
time: 426 us
  waiting for transfers between devices  313 us (73%)
  blocking collectives  67.6 us (16%)
  matrix products  20.8 us (5%)
  between operations  14.3 us (3%)
  other arithmetic  9.62 us (2%)
    reduce_scatter x1, waiting for transfers between devices, local(): lax.psum_scatter(term_query, 'kv', scatter_dimension=0, tiled=True)  64.2 us
    reduce_scatter x1, waiting for transfers between devices, local(): lax.psum_scatter(term_values, 'kv', scatter_dimension=0, tiled=True)  64 us
    psum x1, waiting for transfers between devices, local(): hidden = lax.psum(term_hidden, 'kv').astype(jnp.float32)  56.8 us
    reduce_scatter x1, waiting for transfers between devices, local(): lax.psum_scatter(term_gates, 'kv', scatter_dimension=0, tiled=True)  55.3 us
    reduce_scatter x1, waiting for transfers between devices, local(): lax.psum_scatter(term_keys, 'kv', scatter_dimension=0, tiled=True)  35 us
    psum x1, blocking collectives, local(): total_all = lax.psum(squares_in, 'kv')  22.1 us
    psum x1, blocking collectives, local(): total_mid = lax.psum(squares_mid, 'kv')  21.6 us
    reduce_scatter x1, waiting for transfers between devices, local(): lax.psum_scatter(down_terms.astype(jnp.bfloat16), 'tp', scatter_dimension...  19.4 us
  transfers between devices with their start and end apart: 7, of which 7 were waited for; matrix products, arithmetic and copies ran while one was open for 4% of the time, Pallas kernels for 0%

profile of v1, /device:TPU:0, one launch (start us, length us, event | category | flops | bytes accessed | tf_op | source)
XLA Modules:
  0.0 425.5 jit_solution(82238309147636796)
XLA Ops:
  7.2 6.9 %all_gather.6 = bf16[128,512]{1,0:T(8,128)(2,1)S(1)} all-gather(bf16[32,512]{1,0:T(8,128)(2,1)} %param.13), channel_id=1, replica_groups=mesh['kv'=8,'tp'=4] {'tp'}, dimensions={0}, use_global_device_ids=true | all-gather | bytes 163840 | tf_op jit(solution)/shard_map/all_gather | solution.py:44
  14.1 2.0 convolution_convert_fusion.4
  16.1 1.9 convolution_convert_fusion.5
  18.1 1.7 convolution_convert_fusion.2
  19.9 2.2 convolution_convert_fusion.1
  22.3 0.1 fusion.3
  22.4 22.1 %psum.21 = f32[128]{0:T(128)S(1)} all-reduce(f32[128]{0:T(128)S(1)} %fusion.3), channel_id=1, replica_groups=mesh['kv'=8,'tp'=4] {'kv'}, use_global_device_ids=true, to_apply=%region_2.0 | all-reduce | flops 128 | bytes 1024 | tf_op jit(solution)/shard_map/psum | solution.py:60
  44.5 0.1 multiply_cosine_fusion
  44.7 35.0 %reduce-scatter.9.cloned.1.call-done = bf16[16,512]{1,0:T(8,128)(2,1)} async-done(((bf16[128,512]{1,0:T(8,128)(2,1)}), bf16[16,512]{1,0:T(8,128)(2,1)}) %reduce-scatter.9.cloned.1.call-update) | async-done | bytes 16400 | tf_op jit(solution)/shard_map/reduce_scatter | solution.py:63
  79.7 64.2 %reduce-scatter.7.cloned.1.call-done = bf16[16,512]{1,0:T(8,128)(2,1)} async-done(((bf16[128,512]{1,0:T(8,128)(2,1)}), bf16[16,512]{1,0:T(8,128)(2,1)}) %reduce-scatter.7.cloned.1.call-update) | async-done | bytes 16400 | tf_op jit(solution)/shard_map/reduce_scatter | solution.py:62
  143.9 0.8 convert_multiply_fusion.5
  144.7 0.1 multiply_subtract_fusion
  144.8 0.1 pad_maximum_fusion
  144.9 64.0 %reduce-scatter.11.cloned.1.call-done = bf16[16,1024]{1,0:T(8,128)(2,1)} async-done(((bf16[128,1024]{1,0:T(8,128)(2,1)}), bf16[16,1024]{1,0:T(8,128)(2,1)}) %reduce-scatter.11.cloned.1.call-update) | async-done | bytes 32784 | tf_op jit(solution)/shard_map/reduce_scatter | solution.py:64
  208.9 0.8 convert_multiply_fusion.4
  209.7 4.1 multiply_add_fusion
  213.9 4.1 fusion.14
  218.0 0.1 fusion.12
  218.3 55.3 %reduce-scatter.13.cloned.1.call-done = bf16[16,1024]{1,0:T(8,128)(2,1)} async-done(((bf16[128,1024]{1,0:T(8,128)(2,1)}), bf16[16,1024]{1,0:T(8,128)(2,1)}) %reduce-scatter.13.cloned.1.call-update) | async-done | bytes 32784 | tf_op jit(solution)/shard_map/reduce_scatter | solution.py:65
  273.6 0.9 multiply_convert_fusion.2
  274.5 11.7 %all_to_all.5 = bf16[8,16,1024]{2,1,0:T(8,128)(2,1)S(1)} all-to-all(bf16[8,16,1024]{2,1,0:T(8,128)(2,1)S(1)} %stack.2), channel_id=1, replica_groups=mesh['kv'=8,'tp'=4] {'kv'}, dimensions={0} | all-to-all | bytes 524288 | tf_op jit(solution)/shard_map/all_to_all | solution.py:92
  286.1 1.0 convolution_convert_fusion.6
  287.2 18.0 %reduce-scatter.15.cloned.1.call-done = bf16[32,512]{1,0:T(8,128)(2,1)} async-done(((bf16[128,512]{1,0:T(8,128)(2,1)}), bf16[32,512]{1,0:T(8,128)(2,1)}) %reduce-scatter.15.cloned.1.call-update) | async-done | bytes 32784 | tf_op jit(solution)/shard_map/reduce_scatter | solution.py:103
  305.2 0.8 add_convert_fusion.1
  306.0 5.4 %all_gather.7 = bf16[128,512]{1,0:T(8,128)(2,1)S(1)} all-gather(bf16[32,512]{1,0:T(8,128)(2,1)S(1)} %add_convert_fusion.1), channel_id=1, replica_groups=mesh['kv'=8,'tp'=4] {'tp'}, dimensions={0}, use_global_device_ids=true | all-gather | bytes 163840 | tf_op jit(solution)/shard_map/all_gather | solution.py:107
  311.4 3.9 convolution_convert_fusion
  315.4 0.1 fusion.5
  315.5 21.6 %psum.23 = f32[128]{0:T(128)S(1)} all-reduce(f32[128]{0:T(128)S(1)} %fusion.5), channel_id=1, replica_groups=mesh['kv'=8,'tp'=4] {'kv'}, use_global_device_ids=true, to_apply=%region_10.11 | all-reduce | flops 128 | bytes 1024 | tf_op jit(solution)/shard_map/psum | solution.py:114
  337.1 56.8 %all-reduce.2.cloned.1.call-done = bf16[128,4096]{1,0:T(8,128)(2,1)} async-done(((bf16[128,4096]{1,0:T(8,128)(2,1)}), bf16[128,4096]{1,0:T(8,128)(2,1)}) %all-reduce.2.cloned.1.call-update) | async-done | bytes 1048592 | tf_op jit(solution)/shard_map/psum | solution.py:116
  394.0 3.9 convolution_convert_fusion.3
  397.9 19.4 %reduce-scatter.17.cloned.1.call-done = bf16[32,512]{1,0:T(8,128)(2,1)} async-done(((bf16[128,512]{1,0:T(8,128)(2,1)}), bf16[32,512]{1,0:T(8,128)(2,1)}) %reduce-scatter.17.cloned.1.call-update) | async-done | bytes 32784 | tf_op jit(solution)/shard_map/reduce_scatter | solution.py:119
  417.3 1.4 add_convert_fusion
  (40 shorter events, 0.8 us)
Async XLA Ops:
  7.2 11.0 %copy-start = (bf16[512,1024]{1,0:T(8,128)(2,1)S(1)}, bf16[512,1024]{1,0:T(8,128)(2,1)}, u32[]{:S(2)}) copy-start(bf16[512,1024]{1,0:T(8,128)(2,1)} %param.19) | copy-start | bytes 3145732
  7.2 15.2 %copy-start.6 = (s32[16]{0:T(128)S(1)}, s32[16]{0:T(128)}, u32[]{:S(2)}) copy-start(s32[16]{0:T(128)} %param.14) | copy-start | bytes 196
  7.2 72.5 %reduce-scatter.9.cloned.1.call-start = ((), (), s32[]{:S(2)}) async-start(), calls=%async_computation.8 | async-start | bytes 147456 | tf_op jit(solution)/shard_map/reduce_scatter | solution.py:63
  16.1 127.8 %reduce-scatter.7.cloned.1.call-start = ((), (), s32[]{:S(2)}) async-start(), calls=%async_computation.7 | async-start | bytes 147456 | tf_op jit(solution)/shard_map/reduce_scatter | solution.py:62
  18.1 190.8 %reduce-scatter.11.cloned.1.call-start = ((), (), s32[]{:S(2)}) async-start(), calls=%async_computation.9 | async-start | bytes 294912 | tf_op jit(solution)/shard_map/reduce_scatter | solution.py:64
  19.9 253.7 %reduce-scatter.13.cloned.1.call-start = ((), (), s32[]{:S(2)}) async-start(), calls=%async_computation.10 | async-start | bytes 294912 | tf_op jit(solution)/shard_map/reduce_scatter | solution.py:65
  22.2 283.0 %reduce-scatter.15.cloned.1.call-start = ((), (), s32[]{:S(2)}) async-start(), calls=%async_computation.11 | async-start | bytes 163840 | tf_op jit(solution)/shard_map/reduce_scatter | solution.py:103
  213.9 4.1 copy-start.1
  213.9 59.7 %copy-start.4 = (f32[1024]{0:T(1024)S(1)}, f32[1024]{0:T(1024)}, u32[]{:S(2)}) copy-start(f32[1024]{0:T(1024)} %param.21) | copy-start | bytes 12292
  213.9 72.2 %copy-start.2 = (bf16[1024,512]{1,0:T(8,128)(2,1)S(1)}, bf16[1024,512]{1,0:T(8,128)(2,1)}, u32[]{:S(2)}) copy-start(bf16[1024,512]{1,0:T(8,128)(2,1)} %param.22) | copy-start | bytes 3145732
  213.9 91.3 %copy-start.3 = (bf16[32,512]{1,0:T(8,128)(2,1)S(1)}, bf16[32,512]{1,0:T(8,128)(2,1)}, u32[]{:S(2)}) copy-start(bf16[32,512]{1,0:T(8,128)(2,1)} %param.13) | copy-start | bytes 98308
  213.9 97.5 %copy-start.5 = (f32[512]{0:T(512)S(1)}, f32[512]{0:T(512)}, u32[]{:S(2)}) copy-start(f32[512]{0:T(512)} %param.23) | copy-start | bytes 6148
  287.1 106.9 %all-reduce.2.cloned.1.call-start = ((), (), s32[]{:S(2)}) async-start(), calls=%async_computation.12 | async-start | bytes 2097152 | tf_op jit(solution)/shard_map/psum | solution.py:116
  315.4 101.9 %reduce-scatter.17.cloned.1.call-start = ((), (), s32[]{:S(2)}) async-start(), calls=%async_computation.13 | async-start | bytes 163840 | tf_op jit(solution)/shard_map/reduce_scatter | solution.py:119
Sparse Core Ops, SparseCore 0:
  16.2 63.4 reduce-scatter.8
  83.0 60.8 reduce-scatter.6
  147.8 61.0 reduce-scatter.10
  212.1 61.4 reduce-scatter.12
  287.2 17.9 reduce-scatter.14
  315.5 78.4 all-reduce.1
  398.0 19.2 reduce-scatter.16
